TPU v7x, 32 devices: a whole 2x2x4 slice. The times are simulated.
32 devices in a mesh: grp: 2 (over y), ep: 8 (over z, core), tp: 2 (over x).
Axes of the slice: x: 2, y: 2, z: 4, core: 2. Of those that a mesh axis runs over, the one named last changes fastest.
Arguments:
- tokens: bfloat16 [512, 2048], P(('grp', 'ep')), parts along dimension 0, may hold values from -12 to 12
- routes: int32 [512, 4], P(('grp', 'ep')), parts along dimension 0, may hold values from 0 to 7, all different within a row; in each aligned block of 32 rows (0 to 31, 32 to 63, ...) at most 32 rows name the same one
- gates: float32 [512, 4], P(('grp', 'ep')), parts along dimension 0, may hold values from 0.1 to 1
- norm_gain: bfloat16 [2048], replicated, may hold values from 0.099609375 to 1.8984375
- exp_gate: bfloat16 [8, 2048, 2048], P('ep', None, 'tp'), may hold values from -0.125 to 0.125
- exp_up: bfloat16 [8, 2048, 2048], P('ep', None, 'tp'), may hold values from -0.125 to 0.125
- exp_down: bfloat16 [8, 2048, 2048], P('ep', 'tp'), may hold values from -0.26516504 to 0.26516504
- sh_gate: bfloat16 [2048, 1024], P(None, 'tp'), may hold values from -0.125 to 0.125
- sh_up: bfloat16 [2048, 1024], P(None, 'tp'), may hold values from -0.125 to 0.125
- sh_down: bfloat16 [1024, 2048], P('tp'), may hold values from -0.375 to 0.375
- out_gain: bfloat16 [2048], P('tp'), may hold values from 0.099609375 to 1.8984375
Outputs:
- mixed: bfloat16 [512, 2048], P(('grp', 'ep'), 'tp'), parts along dimension 0
There are 2 independent parts, one for each index of `grp`. A program takes and returns all parts, laid end to end along the dimension named above; an argument that names none is the same for every part. Nothing has to cross between parts.
Inputs may be any that keep to these rules, and one draw needn't show every extreme that they name: `routes`: each row names 4 different experts; within the rows of one device (aligned blocks of 32 rows) no expert is named by more than 32 rows, a bound that some block reaches.
All inputs are finite; a program needn't handle non-finite values.
Results may differ from a plain program's by a relative error of at most 0.015.
Values may be sent and summed in bfloat16 or wider, within the bound.
A program may use at most 64 MiB of HBM per device.

v0:
```python
import jax
import jax.numpy as jnp
from jax import lax
from jax.sharding import PartitionSpec as P

D = 2048


EPSILON = 1e-06


def slot_order(flat_routes, count):
    hits = (flat_routes[:, None] == jnp.arange(count, dtype=jnp.int32)[None, :]).astype(jnp.int32)
    before = jnp.cumsum(hits, axis=0) - hits
    return jnp.sum(before * hits, axis=1)


def slot_tables(position, flat_token, gate_values, slots_all):
    placed = position[:, None] == jnp.arange(slots_all, dtype=jnp.int32)[None, :]
    used = jnp.any(placed, axis=0)
    slot_token = jnp.sum(jnp.where(placed, flat_token[:, None], 0), axis=0)
    slot_gate = jnp.sum(jnp.where(placed, gate_values[:, None], jnp.float32(0.0)), axis=0)
    return (used, slot_token, slot_gate)


def shards(
    tokens, routes, gates, norm_gain, exp_gate, exp_up, exp_down, sh_gate, sh_up, sh_down, out_gain
):
    ep_count = lax.axis_size("ep")
    token_count, top_count = routes.shape
    local_count = exp_gate.shape[0]
    expert_count = local_count * ep_count
    capacity = min(
        token_count, max(2, 2 * ((token_count * top_count + expert_count - 1) // expert_count))
    )
    slots_all = ep_count * local_count * capacity
    values = tokens.astype(jnp.float32)
    normed = (
        values
        * lax.rsqrt(jnp.mean(values * values, axis=1, keepdims=True) + EPSILON)
        * norm_gain.astype(jnp.float32)
    ).astype(jnp.bfloat16)
    flat_expert = routes.reshape(-1)
    slot_index = slot_order(flat_expert, expert_count)
    flat_token = jnp.repeat(jnp.arange(token_count, dtype=jnp.int32), top_count)
    position = flat_expert * capacity + slot_index
    used, slot_token, slot_gate = slot_tables(position, flat_token, gates.reshape(-1), slots_all)
    send = jnp.where(used[:, None], normed[slot_token], jnp.zeros((), jnp.bfloat16))
    send = send.reshape(ep_count, local_count, capacity, normed.shape[1])
    received = lax.all_to_all(send, "ep", split_axis=0, concat_axis=0, tiled=True)
    gate_act = jnp.einsum("secd,edf->secf", received, exp_gate, preferred_element_type=jnp.float32)
    up_act = jnp.einsum("secd,edf->secf", received, exp_up, preferred_element_type=jnp.float32)
    hidden = (jax.nn.silu(gate_act) * up_act).astype(jnp.bfloat16)
    expert_part = jnp.einsum("secf,efd->secd", hidden, exp_down, preferred_element_type=jnp.float32)
    shared_gate = jnp.dot(normed, sh_gate, preferred_element_type=jnp.float32)
    shared_up = jnp.dot(normed, sh_up, preferred_element_type=jnp.float32)
    shared_hidden = (jax.nn.silu(shared_gate) * shared_up).astype(jnp.bfloat16)
    shared_part = jnp.dot(shared_hidden, sh_down, preferred_element_type=jnp.float32)
    expert_sum, shared_sum = (
        lax.psum_scatter(
            expert_part.astype(jnp.bfloat16), "tp", scatter_dimension=3, tiled=True
        ).astype(jnp.float32),
        lax.psum_scatter(
            shared_part.astype(jnp.bfloat16), "tp", scatter_dimension=1, tiled=True
        ).astype(jnp.float32),
    )
    expert_rows = expert_sum.astype(jnp.bfloat16)
    shared_values = lax.optimization_barrier(shared_sum.astype(jnp.bfloat16)).astype(jnp.float32)
    feature_count = expert_rows.shape[3]
    returned = lax.all_to_all(expert_rows, "ep", split_axis=0, concat_axis=0, tiled=True)
    pair_rows = returned.reshape(slots_all, feature_count)[position].astype(jnp.float32)
    routed = jnp.sum(
        gates[:, :, None] * pair_rows.reshape(token_count, top_count, feature_count), axis=1
    )
    total = routed + shared_values
    squares = jnp.sum(total * total, axis=1)
    whole_squares = lax.psum(squares, "tp")
    scale = lax.rsqrt(whole_squares / D + EPSILON)
    return (total * scale[:, None] * out_gain.astype(jnp.float32)).astype(jnp.bfloat16)


def solution(mesh):
    placed = (
        P(("grp", "ep"), None),
        P(("grp", "ep"), None),
        P(("grp", "ep"), None),
        P(),
        P("ep", None, "tp"),
        P("ep", None, "tp"),
        P("ep", "tp", None),
        P(None, "tp"),
        P(None, "tp"),
        P("tp", None),
        P("tp"),
    )
    return jax.shard_map(
        shards, mesh=mesh, in_specs=placed, out_specs=P(("grp", "ep"), "tp"), check_vma=False
    )
```

profile of v0, /device:TPU:0, one launch (start us, length us, event | category | flops | bytes accessed | tf_op | source)
XLA Modules:
  0.0 109.7 jit_solution(1442257461080784481)
XLA Ops:
  6.5 0.0 copy-start
  6.5 0.0 reduce-scatter.3.cloned.1.call-start
  6.5 1.2 %fusion.35 = f32[32]{0:T(128)S(1)} fusion(bf16[32,2048]{1,0:T(8,128)(2,1)} %param.11), kind=kLoop, calls=%fused_computation.25 | loop fusion | flops 196576 | bytes 131200 | tf_op jit(solution)/shard_map/reduce_sum | solution.py:40
  7.7 0.7 convert_element_type.55
  8.4 0.8 copy.24
  9.2 0.1 reshape.109
  9.3 0.1 broadcast_in_dim.45
  9.4 0.1 fusion.44
  9.5 0.2 reduce_window_sum.11
  9.7 0.2 select_reduce_fusion.1
  9.9 0.1 fusion.38
  10.0 0.1 select_reduce_fusion
  10.1 0.1 broadcast_in_dim.42
  10.2 1.0 fusion.37
  11.2 1.4 %gather_fusion = bf16[256,2048]{1,0:T(8,128)(2,1)S(1)} fusion(bf16[32,2048]{1,0:T(8,128)(2,1)S(1)} %fusion.37, s32[1024]{0:T(1024)S(1)} %pad_clamp_fusion.1), kind=kCustom, calls=%fused_computation | custom fusion | bytes 2098176 | tf_op jit(solution)/shard_map/gather | solution.py:48
  12.6 0.0 copy-start.5
  12.6 0.1 broadcast_select_fusion
  12.7 33.0 %all_to_all.10 = bf16[8,1,32,2048]{3,2,1,0:T(8,128)(2,1)S(1)} all-to-all(bf16[8,1,32,2048]{3,2,1,0:T(8,128)(2,1)S(1)} %broadcast_select_fusion), channel_id=1, replica_groups=mesh['grp'=2,'ep'=8,'tp'=2] {'ep'}, dimensions={0} | all-to-all | bytes 2097152 | tf_op jit(solution)/shard_map/all_to_all | solution.py:50
  45.7 0.0 copy-done.5
  45.7 2.3 %fusion.12 = f32[8,1,32,1024]{3,2,0,1:T(8,128)} fusion(bf16[1,2048,1024]{2,1,0:T(8,128)(2,1)S(1)} %copy-done.5, bf16[8,1,32,2048]{3,2,1,0:T(8,128)(2,1)S(1)} %all_to_all.10), kind=kOutput, calls=%fused_computation.11 | convolution fusion | flops 1073741824 | bytes 6291456 | tf_op jit(solution)/shard_map/secd,edf->secf/dot_general | solution.py:51
  48.0 7.2 %fusion.9 = bf16[8,1,32,2048]{3,2,0,1:T(8,128)(2,1)} fusion(bf16[1,1024,2048]{2,1,0:T(8,128)(2,1)} %param.17, bf16[1,2048,1024]{2,1,0:T(8,128)(2,1)} %param.16, bf16[8,1,32,2048]{3,2,1,0:T(8,128)(2,1)S(1)} %all_to_all.10, f32[8,1,32,1024]{3,2,0,1:T(8,128)} %fusion.12), kind=kOutput, calls=%fused_computation.9 | convolution fusion | flops 2149580800 | bytes 11534336 | tf_op jit(solution)/shard_map/secf,efd->secd/dot_general | solution.py:54
  55.3 0.0 reduce-scatter.3.cloned.1.call-update
  55.3 19.5 %reduce-scatter.3.cloned.1.call-done = bf16[8,1,32,1024]{3,2,0,1:T(8,128)(2,1)} async-done(((bf16[8,1,32,2048]{3,2,0,1:T(8,128)(2,1)}), bf16[8,1,32,1024]{3,2,0,1:T(8,128)(2,1)}) %reduce-scatter.3.cloned.1.call-update) | async-done | bytes 524304 | tf_op jit(solution)/shard_map/reduce_scatter | solution.py:60
  74.8 4.6 %all-to-all-start.1 = ((bf16[8,1,32,1024]{3,2,1,0:T(8,128)(2,1)}), bf16[8,1,32,1024]{3,2,1,0:T(8,128)(2,1)S(1)}, u32[]{:S(2)}, u32[]{:S(2)}) async-start(bf16[8,1,32,1024]{3,2,1,0:T(8,128)(2,1)} %bitcast.85), calls=%async_computation.2 | async-start | bytes 1048576 | tf_op jit(solution)/shard_map/all_to_all | solution.py:70
  79.4 0.0 reduce-scatter.5.cloned.1.call-start
  79.4 2.0 %fusion.49 = f32[32,512]{1,0:T(8,128)S(1)} fusion(bf16[32,2048]{1,0:T(8,128)(2,1)S(1)} %fusion.37, bf16[2048,512]{1,0:T(8,128)(2,1)} %param.18), kind=kOutput, calls=%fused_computation.55 | convolution fusion | flops 67108864 | bytes 2293760 | tf_op jit(solution)/shard_map/dot_general | solution.py:55
  81.5 0.0 copy-done
  81.5 0.0 copy-start.3
  81.5 0.0 copy-start.2
  81.5 0.0 copy-start.4
  81.5 3.2 %convolution_convert_fusion = bf16[32,2048]{1,0:T(8,128)(2,1)} fusion(bf16[512,2048]{1,0:T(8,128)(2,1)S(1)} %copy-done, bf16[32,2048]{1,0:T(8,128)(2,1)S(1)} %fusion.37, bf16[2048,512]{1,0:T(8,128)(2,1)} %param.19, f32[32,512]{1,0:T(8,128)S(1)} %fusion.49), kind=kOutput, calls=%fused_computation.10 | convolution fusion | flops 134381568 | bytes 4521984 | tf_op jit(solution)/shard_map/dot_general | solution.py:58
  84.7 0.0 reduce-scatter.5.cloned.1.call-update
  84.7 0.0 copy-done.3
  84.7 0.0 copy-done.2
  84.7 0.1 copy.27
  84.8 0.1 mul.99
  84.9 0.0 copy-done.4
  84.9 0.1 copy.23
  85.0 10.6 %reduce-scatter.5.cloned.1.call-done = bf16[32,1024]{1,0:T(8,128)(2,1)} async-done(((bf16[32,2048]{1,0:T(8,128)(2,1)}), bf16[32,1024]{1,0:T(8,128)(2,1)}) %reduce-scatter.5.cloned.1.call-update) | async-done | bytes 65552 | tf_op jit(solution)/shard_map/reduce_scatter | solution.py:63
  95.6 0.0 copy-start.1
  95.6 0.0 all-to-all-done.1
  95.6 0.9 gather_fusion.1
  96.5 0.2 reshape.116
  96.7 0.4 multiply_reduce_fusion
  97.1 0.0 copy-done.1
  97.1 0.1 multiply_reduce_fusion.1
  97.2 4.9 %psum.7 = f32[32]{0:T(128)S(1)} all-reduce(f32[32]{0:T(128)S(1)} %multiply_reduce_fusion.1), channel_id=1, replica_groups=mesh['grp'=2,'ep'=8,'tp'=2] {'tp'}, use_global_device_ids=true, to_apply=%region_9.10 | all-reduce | flops 32 | bytes 256 | tf_op jit(solution)/shard_map/psum | solution.py:77
  102.2 0.7 multiply_convert_fusion
  (10 shorter events, 0.1 us)
Async XLA Ops:
  6.5 74.9 %copy-start = (bf16[512,2048]{1,0:T(8,128)(2,1)S(1)}, bf16[512,2048]{1,0:T(8,128)(2,1)}, u32[]{:S(2)}) copy-start(bf16[512,2048]{1,0:T(8,128)(2,1)} %param.20) | copy-start | bytes 6291460
  6.5 68.2 %reduce-scatter.3.cloned.1.call-start = ((), (), s32[]{:S(2)}) async-start(), calls=%async_computation.4 | async-start | bytes 1572864 | tf_op jit(solution)/shard_map/reduce_scatter | solution.py:60
  12.6 33.1 %copy-start.5 = (bf16[1,2048,1024]{2,1,0:T(8,128)(2,1)S(1)}, bf16[1,2048,1024]{2,1,0:T(8,128)(2,1)}, u32[]{:S(2)}) copy-start(bf16[1,2048,1024]{2,1,0:T(8,128)(2,1)} %param.15) | copy-start | bytes 12582916
  74.8 20.9 %all-to-all-start.1 = ((bf16[8,1,32,1024]{3,2,1,0:T(8,128)(2,1)}), bf16[8,1,32,1024]{3,2,1,0:T(8,128)(2,1)S(1)}, u32[]{:S(2)}, u32[]{:S(2)}) async-start(bf16[8,1,32,1024]{3,2,1,0:T(8,128)(2,1)} %bitcast.85), calls=%async_computation.2 | async-start | bytes 1048576 | tf_op jit(solution)/shard_map/all_to_all | solution.py:70
  79.4 16.3 %reduce-scatter.5.cloned.1.call-start = ((), (), s32[]{:S(2)}) async-start(), calls=%async_computation.5 | async-start | bytes 196608 | tf_op jit(solution)/shard_map/reduce_scatter | solution.py:63
  81.5 3.2 %copy-start.3 = (bf16[1024]{0:T(1024)(128)(2,1)S(1)}, bf16[1024]{0:T(1024)(128)(2,1)}, u32[]{:S(2)}) copy-start(bf16[1024]{0:T(1024)(128)(2,1)} %param.21) | copy-start | bytes 6148
  81.5 3.2 %copy-start.2 = (s32[32,4]{0,1:T(4,128)S(1)}, s32[32,4]{0,1:T(4,128)}, u32[]{:S(2)}) copy-start(s32[32,4]{0,1:T(4,128)} %param.12) | copy-start | bytes 1540
  81.5 3.4 %copy-start.4 = (f32[32,4]{0,1:T(4,128)S(1)}, f32[32,4]{0,1:T(4,128)}, u32[]{:S(2)}) copy-start(f32[32,4]{0,1:T(4,128)} %param.13) | copy-start | bytes 1540
  95.6 1.4 %copy-start.1 = (bf16[32,1024]{1,0:T(8,128)(2,1)S(1)}, bf16[32,1024]{1,0:T(8,128)(2,1)}, u32[]{:S(2)}) copy-start(bf16[32,1024]{1,0:T(8,128)(2,1)} %reduce-scatter.5.cloned.1.call-done) | copy-start | bytes 196612
Sparse Core Ops, SparseCore 0:
  55.4 19.3 reduce-scatter.2
  84.8 10.8 reduce-scatter.4
where the time goes:
time: 110 us
  blocking collectives  37.9 us (34%)
  waiting for transfers between devices  30.1 us (27%)
  matrix products  14.7 us (13%)
  between operations  13.6 us (12%)
  other arithmetic  4.97 us (5%)
  starting transfers between devices  4.65 us (4%)
  local copies, waits for them, and re-layouts  3.77 us (3%)
    all_to_all x1, blocking collectives, shards(): lax.all_to_all(send, 'ep', split_axis=0, concat_axis=0, tiled=True)  33 us
    reduce_scatter x1, waiting for transfers between devices, shards(): lax.psum_scatter(expert_part.astype(jnp.bfloat16), 'tp', scatter_dimensio...  19.5 us
    reduce_scatter x1, waiting for transfers between devices, shards(): lax.psum_scatter(shared_part.astype(jnp.bfloat16), 'tp', scatter_dimensio...  10.6 us
    dot_general x1, matrix products, shards(): jnp.einsum('secf,efd->secd', hidden, exp_down, preferred_element_type=jnp...  7.21 us
    psum x1, blocking collectives, shards(): whole_squares = lax.psum(squares, 'tp')  4.93 us
    all_to_all x1, starting transfers between devices, shards(): lax.all_to_all(expert_rows, 'ep', split_axis=0, concat_axis=0, tiled=True)  4.61 us
    dot_general x1, matrix products, shards(): jnp.dot(shared_hidden, sh_down, preferred_element_type=jnp.float32)  3.15 us
    dot_general x1, matrix products, shards(): jnp.einsum('secd,edf->secf', received, exp_gate, preferred_element_type=j...  2.33 us
  transfers between devices with their start and end apart: 3, of which 2 were waited for; matrix products, arithmetic and copies ran while one was open for 5% of the time, Pallas kernels for 0%

commit v1 on v0

v1 whole, which is shorter than its diff:
```python
import functools

import jax
import jax.numpy as jnp
from jax import lax
from jax.experimental import pallas as pl
from jax.experimental.pallas import tpu as pltpu
from jax.sharding import PartitionSpec as P

EPSILON = 1e-06
MESH = pl.DeviceIdType.MESH
F32 = jnp.float32
BF16 = jnp.bfloat16


def silu(v):
    return v / (1.0 + jnp.exp(-v))


def kernel(
    n_ep, n_tp, experts,
    tok_ref, routes_ref, gates_ref, ngain_ref, wg_hbm, wu_hbm, wd_hbm, sg_hbm, su_hbm, sd_hbm, ogain_ref,
    out_ref,
    wg, wu, wd, sg, su, sd, xs, hid, shid, shp, d_out, d_in, x_out, x_in, acc, z_out, z_in, q_out, q_in,
    w_sem, disp_send, disp_recv, fwd_send, fwd_recv, d_send, d_recv, x_send, x_recv, z_send, z_recv, q_send, q_recv,
):
    nz = n_ep // 2
    me = lax.axis_index("ep")
    t = lax.axis_index("tp")
    z, c = me // 2, lax.rem(me, 2)
    other = 1 - c
    T, D = tok_ref.shape
    F = wg.shape[1]
    S = sg.shape[1]
    Dt = D // n_tp
    rows = nz * T
    pad = xs.shape[3] - D

    loads = []
    for i, (src, dst) in enumerate(
        ((sg_hbm, sg), (su_hbm, su), (sd_hbm, sd), (wg_hbm.at[0], wg), (wu_hbm.at[0], wu), (wd_hbm.at[0], wd))
    ):
        copy = pltpu.make_async_copy(src, dst, w_sem.at[i])
        copy.start()
        loads.append(copy)

    def zpeer(dz):
        return lax.rem(z + dz, nz)

    def tpeer(j):
        return lax.rem(t + j, n_tp)

    partner = {"ep": z * 2 + other}
    barrier = pltpu.get_barrier_semaphore()
    peers = [{"ep": zpeer(dz) * 2 + c} for dz in range(1, nz)] + [partner]
    peers += [{"tp": tpeer(j)} for j in range(1, n_tp)]
    for peer in peers:
        pl.semaphore_signal(barrier, inc=1, device_id=peer, device_id_type=MESH)

    def remote(src, dst, ssem, rsem, device):
        return pltpu.make_async_remote_copy(
            src_ref=src, dst_ref=dst, send_sem=ssem, recv_sem=rsem, device_id=device, device_id_type=MESH
        )

    values = tok_ref[...].astype(F32)
    scale = lax.rsqrt(jnp.mean(values * values, axis=1, keepdims=True) + EPSILON)
    normed = (values * scale * ngain_ref[...].astype(F32)).astype(BF16)
    lane = lax.broadcasted_iota(jnp.int32, (T, pad), 1)
    lane_expert = lax.rem(lane, experts)
    dense = jnp.zeros((T, pad), F32)
    for k in range(routes_ref.shape[1]):
        dense = dense + jnp.where(lane_expert == routes_ref[:, k : k + 1], gates_ref[:, k : k + 1], 0.0)
    high = dense.astype(BF16).astype(F32)
    rest = dense - high
    mid = rest.astype(BF16).astype(F32)
    part = lane // experts
    packed = jnp.where(part == 0, high, jnp.where(part == 1, mid, jnp.where(part == 2, rest - mid, 0.0)))
    xs[c, z, :, :D] = normed
    xs[c, z, :, D:] = packed.astype(BF16)

    pl.semaphore_wait(barrier, len(peers))

    own = xs.at[c, z]
    sends = []
    order = sorted(range(1, nz), key=lambda d: -min(d, nz - d))
    for dz in order:
        copy = remote(own, own, disp_send.at[dz], disp_recv.at[dz], {"ep": zpeer(dz) * 2 + c})
        copy.start()
        sends.append(copy)
    first = remote(own, own, fwd_send.at[0], fwd_recv.at[0], partner)
    first.start()

    loads[0].wait()
    loads[1].wait()
    tile = min(256, S)

    @pl.loop(0, S // tile)
    def _(i):
        cols = pl.ds(pl.multiple_of(i * tile, tile), tile)
        x = xs[c, z, :, :D]
        g = jnp.dot(x, sg[:, cols], preferred_element_type=F32)
        u = jnp.dot(x, su[:, cols], preferred_element_type=F32)
        shid[:, cols] = (silu(g) * u).astype(BF16)

    loads[2].wait()
    dtile = min(256, Dt)

    @pl.loop(0, D // dtile)
    def _(i):
        cols = pl.ds(pl.multiple_of(i * dtile, dtile), dtile)
        shp[:, cols] = jnp.dot(shid[...], sd[:, cols], preferred_element_type=F32)

    forwards = [first]
    for dz in range(1, nz):
        src_z = lax.rem(z - dz + nz, nz)
        block = xs.at[c, src_z]
        remote(block, block, disp_send.at[dz], disp_recv.at[dz], partner).wait_recv()
        copy = remote(block, block, fwd_send.at[dz], fwd_recv.at[dz], partner)
        copy.start()
        forwards.append(copy)

    loads[3].wait()
    loads[4].wait()
    ftile = min(256, F)
    glane = lax.broadcasted_iota(jnp.int32, (rows, pad), 1)
    mine = (lax.rem(glane, experts) == me) & (glane < 3 * experts)

    def hidden(half, slot):
        packed_gates = xs[half, :, :, D:].reshape(rows, pad).astype(F32)
        weight = jnp.sum(jnp.where(mine, packed_gates, 0.0), axis=1, keepdims=True)

        @pl.loop(0, F // ftile)
        def _(i):
            cols = pl.ds(pl.multiple_of(i * ftile, ftile), ftile)
            x = xs[half, :, :, :D].reshape(rows, D)
            g = jnp.dot(x, wg[:, cols], preferred_element_type=F32)
            u = jnp.dot(x, wu[:, cols], preferred_element_type=F32)
            hid[slot, :, cols] = (silu(g) * u * weight).astype(BF16)

    hidden(c, 0)
    for dz in range(nz):
        src_z = lax.rem(z - dz + nz, nz)
        block = xs.at[other, src_z]
        remote(block, block, fwd_send.at[dz], fwd_recv.at[dz], partner).wait_recv()
    hidden(other, 1)
    loads[5].wait()

    def down(slot, tp, store):
        @pl.loop(0, Dt // dtile)
        def _(i):
            src = pl.ds(pl.multiple_of(tp * Dt + i * dtile, dtile), dtile)
            dst = pl.ds(pl.multiple_of(i * dtile, dtile), dtile)
            store(src, dst, jnp.dot(hid[slot], wd[:, src], preferred_element_type=F32))

    js = list(range(1, n_tp)) + [0]
    d_copies = {}
    for j in js:
        def store(src, dst, value):
            d_out[j, :, :, dst] = value.astype(BF16).reshape(nz, T, dtile)

        down(1, tpeer(j), store)
        copy = remote(d_out.at[j], d_in.at[j], d_send.at[j], d_recv.at[j], partner)
        copy.start()
        d_copies[j] = copy

    x_copies = {}
    for j in js:
        def keep(src, dst, value):
            acc[:, :, dst] = value.reshape(nz, T, dtile)
            acc[z, :, dst] += shp[:, src]

        down(0, tpeer(j), keep)
        d_copies[j].wait_recv()
        if j == 0:
            acc[...] += d_in[j].astype(F32)
        else:
            for dz in order + [0]:
                zt = zpeer(dz)
                x_out[j, zt] = (acc[zt] + d_in[j, zt].astype(F32)).astype(BF16)
                copy = remote(
                    x_out.at[j, zt], x_in.at[j, zt], x_send.at[j, dz], x_recv.at[j, dz], {"tp": tpeer(j)}
                )
                copy.start()
                x_copies[j, dz] = copy

    z_copies = {}
    for dz in order + [0]:
        zt = zpeer(dz)
        total = acc[zt]
        for j in range(1, n_tp):
            x_copies[j, dz].wait_recv()
            total = total + x_in[j, zt].astype(F32)
        if dz == 0:
            acc[zt] = total
        else:
            z_out[dz] = total.astype(BF16)
            copy = remote(z_out.at[dz], z_in.at[dz], z_send.at[dz], z_recv.at[dz], {"ep": zt * 2 + c})
            copy.start()
            z_copies[dz] = copy

    total = acc[z]
    for dz in range(1, nz):
        z_copies[dz].wait_recv()
        total = total + z_in[dz].astype(F32)
    squares = jnp.sum(total * total, axis=1, keepdims=True)
    q_out[...] = jnp.broadcast_to(squares, q_out.shape)
    q_copies = []
    for j in range(1, n_tp):
        copy = remote(q_out, q_in.at[j], q_send.at[j], q_recv.at[j], {"tp": tpeer(j)})
        copy.start()
        q_copies.append(copy)
    gained = total * ogain_ref[...].astype(F32)
    for j, copy in enumerate(q_copies):
        copy.wait_recv()
        squares = squares + q_in[j + 1, :, :1]
    out_ref[...] = (gained * lax.rsqrt(squares / D + EPSILON)).astype(BF16)

    for copy in sends + forwards + list(d_copies.values()) + list(x_copies.values()) + list(z_copies.values()) + q_copies:
        copy.wait_send()


def solution(mesh):
    n_ep, n_tp = mesh.shape["ep"], mesh.shape["tp"]
    nz = n_ep // 2

    def shards(tokens, routes, gates, norm_gain, exp_gate, exp_up, exp_down, sh_gate, sh_up, sh_down, out_gain):
        T, D = tokens.shape
        local, _, F = exp_gate.shape
        S = sh_gate.shape[1]
        assert local == 1
        experts = local * n_ep
        Dt = D // n_tp
        pad = 128 * ((3 * experts + 127) // 128)
        vmem = pl.BlockSpec(memory_space=pltpu.VMEM)
        hbm = pl.BlockSpec(memory_space=pl.ANY)
        dma = pltpu.SemaphoreType.DMA
        return pl.pallas_call(
            functools.partial(kernel, n_ep, n_tp, experts),
            out_shape=jax.ShapeDtypeStruct((T, Dt), BF16),
            in_specs=[vmem] * 4 + [hbm] * 6 + [vmem],
            out_specs=vmem,
            scratch_shapes=[
                pltpu.VMEM((D, F), BF16),
                pltpu.VMEM((D, F), BF16),
                pltpu.VMEM((F, D), BF16),
                pltpu.VMEM((D, S), BF16),
                pltpu.VMEM((D, S), BF16),
                pltpu.VMEM((S, D), BF16),
                pltpu.VMEM((2, nz, T, D + pad), BF16),
                pltpu.VMEM((2, nz * T, F), BF16),
                pltpu.VMEM((T, S), BF16),
                pltpu.VMEM((T, D), F32),
                pltpu.VMEM((n_tp, nz, T, Dt), BF16),
                pltpu.VMEM((n_tp, nz, T, Dt), BF16),
                pltpu.VMEM((n_tp, nz, T, Dt), BF16),
                pltpu.VMEM((n_tp, nz, T, Dt), BF16),
                pltpu.VMEM((nz, T, Dt), F32),
                pltpu.VMEM((nz, T, Dt), BF16),
                pltpu.VMEM((nz, T, Dt), BF16),
                pltpu.VMEM((T, 128), F32),
                pltpu.VMEM((n_tp, T, 128), F32),
                dma((6,)),
                dma((nz,)), dma((nz,)), dma((nz,)), dma((nz,)),
                dma((n_tp,)), dma((n_tp,)),
                dma((n_tp, nz)), dma((n_tp, nz)),
                dma((nz,)), dma((nz,)),
                dma((n_tp,)), dma((n_tp,)),
            ],
            compiler_params=pltpu.CompilerParams(collective_id=0, has_side_effects=True),
        )(
            tokens, routes, gates, norm_gain.reshape(1, -1), exp_gate, exp_up, exp_down,
            sh_gate, sh_up, sh_down, out_gain.reshape(1, -1),
        )

    placed = (
        P(("grp", "ep"), None),
        P(("grp", "ep"), None),
        P(("grp", "ep"), None),
        P(),
        P("ep", None, "tp"),
        P("ep", None, "tp"),
        P("ep", "tp", None),
        P(None, "tp"),
        P(None, "tp"),
        P("tp", None),
        P("tp"),
    )
    return jax.shard_map(
        shards, mesh=mesh, in_specs=placed, out_specs=P(("grp", "ep"), "tp"), check_vma=False
    )
```

time: 110 us -> 46.8 us (0.43)
  Pallas kernels: 0 us -> 39.7 us
  blocking collectives: 37.9 us -> 0 us
  waiting for transfers between devices: 30.1 us -> 0 us
  matrix products: 14.7 us -> 0 us
  between operations: 13.6 us -> 0.01 us
  other arithmetic: 4.97 us -> 0 us
  starting transfers between devices: 4.65 us -> 0 us
  local copies, waits for them, and re-layouts: 3.77 us -> 6.77 us
    pallas_call x0 -> x1, Pallas kernels: none -> 39.7 us  [shards(): pl.pallas_call(functools.partial(kernel, n_ep, n_tp, experts), out_shape=...]
    all_to_all x1 -> x0, blocking collectives: 33 us -> none  [shards(): lax.all_to_all(send, 'ep', split_axis=0, concat_axis=0, tiled=True)]
    reduce_scatter x2 -> x0, waiting for transfers between devices: 30.1 us -> none  [the longest x1 19.5 us: shards(): lax.psum_scatter(expert_part.astype(jnp.bfloat16), 'tp', scatter_dimensio...]
    dot_general x4 -> x0, matrix products: 14.7 us -> none  [the longest x1 7.21 us: shards(): jnp.einsum('secf,efd->secd', hidden, exp_down, preferred_element_type=jnp...]
    psum x1 -> x0, blocking collectives: 4.93 us -> none  [shards(): whole_squares = lax.psum(squares, 'tp')]
    all_to_all x1 -> x0, starting transfers between devices: 4.61 us -> none  [shards(): lax.all_to_all(expert_rows, 'ep', split_axis=0, concat_axis=0, tiled=True)]
    unnamed x14 -> x3, local copies, waits for them, and re-layouts: 0.89 us -> 4.2 us
    convert_element_type x5 -> x0, other arithmetic: 2.51 us -> none  [the longest x1 1 us: shards(): normed = (values * lax.rsqrt(jnp.mean(values * values, axis=1, keepdims=T...]
  transfers between devices with their start and end apart: 3 -> 0, of which waited for: 2 -> 0; matrix products, arithmetic and copies ran while one was open for 5% -> 0% of each run, Pallas kernels for 0% -> 0%
where the time goes in v1:
time: 46.8 us; the launch traced here: 46.5 us
  Pallas kernels  39.7 us (85%)
  local copies, waits for them, and re-layouts  6.77 us (14%)
    pallas_call x1, Pallas kernels, shards(): pl.pallas_call(functools.partial(kernel, n_ep, n_tp, experts), out_shape=...  39.7 us
    unnamed x3, local copies, waits for them, and re-layouts  4.2 us
    reshape x1, local copies, waits for them, and re-layouts, shards(): norm_gain.reshape(1, -1)  1.29 us
    reshape x1, local copies, waits for them, and re-layouts, shards(): out_gain.reshape(1, -1)  1.28 us

profile of v1, /device:TPU:0, one launch (start us, length us, event | category | flops | bytes accessed | tf_op | source)
XLA Modules:
  0.0 46.5 jit_solution(3963664373282921593)
XLA Ops:
  0.0 1.3 %reshape.7.ogain_ref = bf16[1,1024]{1,0:T(2,128)(2,1)} reshape(bf16[1024]{0:T(1024)(128)(2,1)} %param.21) | data formatting | bytes 4096 | tf_op jit(solution)/shard_map/reshape | solution.py:272
  1.3 1.3 %reshape.6.ngain_ref = bf16[1,2048]{1,0:T(2,128)(2,1)} reshape(bf16[2048]{0:T(1024)(128)(2,1)} %param.14) | data formatting | bytes 8192 | tf_op jit(solution)/shard_map/reshape | solution.py:271
  2.6 1.4 %copy.12.routes_ref = s32[32,4]{1,0:T(8,128)} copy(s32[32,4]{0,1:T(4,128)} %param.12) | data formatting | bytes 1024 | tf_op args[1]
  3.9 1.4 %copy.13.gates_ref = f32[32,4]{1,0:T(8,128)} copy(f32[32,4]{0,1:T(4,128)} %param.13) | data formatting | bytes 1024 | tf_op args[2]
  5.3 39.7 %shard_map.109 = bf16[32,1024]{1,0:T(8,128)(2,1)} custom-call(bf16[32,2048]{1,0:T(8,128)(2,1)} %tok_ref.1, s32[32,4]{1,0:T(8,128)} %copy.12.routes_ref, f32[32,4]{1,0:T(8,128)} %copy.13.gates_ref, bf16[1,2048]{1,0:T(2,128)(2,1)} %reshape.6.ngain_ref, bf16[1,2048,1024]{2,1,0:T(8,128)(2,1)} %wg_hbm.1, bf16[1,2048,1024]{2,1,0:T(8,128)(2,1)} %wu_hbm.1, ...), custom_call_target="tpu_custom_call" | custom-call | tf_op jit(solution)/shard_map/pallas_call | solution.py:237
  45.0 1.5 %copy.15 = bf16[32,1024]{1,0:T(8,128)(2,1)} copy(bf16[32,1024]{1,0:T(8,128)(2,1)} %shard_map.109) | data formatting | bytes 131072

commit v2 on v1

--- a/solution.py
+++ b/solution.py
@@ -45,7 +45,11 @@
         loads.append(copy)
 
     def zpeer(dz):
-        return lax.rem(z + dz, nz)
+        peer = z
+        for bit in range(dz.bit_length()):
+            if dz >> bit & 1:
+                peer = peer + (1 << bit) * (1 - 2 * lax.rem(z // (1 << bit), 2))
+        return peer
 
     def tpeer(j):
         return lax.rem(t + j, n_tp)
@@ -64,17 +68,18 @@
 
     values = tok_ref[...].astype(F32)
     scale = lax.rsqrt(jnp.mean(values * values, axis=1, keepdims=True) + EPSILON)
-    normed = (values * scale * ngain_ref[...].astype(F32)).astype(BF16)
-    lane = lax.broadcasted_iota(jnp.int32, (T, pad), 1)
-    lane_expert = lax.rem(lane, experts)
-    dense = jnp.zeros((T, pad), F32)
-    for k in range(routes_ref.shape[1]):
-        dense = dense + jnp.where(lane_expert == routes_ref[:, k : k + 1], gates_ref[:, k : k + 1], 0.0)
+    normed = (values * scale * ngain_ref[...].astype(F32).reshape(1, D)).astype(BF16)
+    row = lax.broadcasted_iota(jnp.int32, (pad, T), 0)
+    row_expert = lax.rem(row, experts)
+    dense = jnp.zeros((pad, T), F32)
+    for k in range(routes_ref.shape[0]):
+        dense = dense + jnp.where(row_expert == routes_ref[k : k + 1, :], gates_ref[k : k + 1, :], 0.0)
     high = dense.astype(BF16).astype(F32)
     rest = dense - high
     mid = rest.astype(BF16).astype(F32)
-    part = lane // experts
+    part = row // experts
     packed = jnp.where(part == 0, high, jnp.where(part == 1, mid, jnp.where(part == 2, rest - mid, 0.0)))
+    packed = packed.T
     xs[c, z, :, :D] = normed
     xs[c, z, :, D:] = packed.astype(BF16)
 
@@ -82,7 +87,7 @@
 
     own = xs.at[c, z]
     sends = []
-    order = sorted(range(1, nz), key=lambda d: -min(d, nz - d))
+    order = list(range(nz - 1, 0, -1))
     for dz in order:
         copy = remote(own, own, disp_send.at[dz], disp_recv.at[dz], {"ep": zpeer(dz) * 2 + c})
         copy.start()
@@ -112,7 +117,7 @@
 
     forwards = [first]
     for dz in range(1, nz):
-        src_z = lax.rem(z - dz + nz, nz)
+        src_z = zpeer(dz)
         block = xs.at[c, src_z]
         remote(block, block, disp_send.at[dz], disp_recv.at[dz], partner).wait_recv()
         copy = remote(block, block, fwd_send.at[dz], fwd_recv.at[dz], partner)
@@ -139,7 +144,7 @@
 
     hidden(c, 0)
     for dz in range(nz):
-        src_z = lax.rem(z - dz + nz, nz)
+        src_z = zpeer(dz)
         block = xs.at[other, src_z]
         remote(block, block, fwd_send.at[dz], fwd_recv.at[dz], partner).wait_recv()
     hidden(other, 1)
@@ -209,7 +214,7 @@
         copy = remote(q_out, q_in.at[j], q_send.at[j], q_recv.at[j], {"tp": tpeer(j)})
         copy.start()
         q_copies.append(copy)
-    gained = total * ogain_ref[...].astype(F32)
+    gained = total * ogain_ref[...].astype(F32).reshape(1, Dt)
     for j, copy in enumerate(q_copies):
         copy.wait_recv()
         squares = squares + q_in[j + 1, :, :1]
@@ -268,8 +273,8 @@
             ],
             compiler_params=pltpu.CompilerParams(collective_id=0, has_side_effects=True),
         )(
-            tokens, routes, gates, norm_gain.reshape(1, -1), exp_gate, exp_up, exp_down,
-            sh_gate, sh_up, sh_down, out_gain.reshape(1, -1),
+            tokens, routes.T, gates.T, norm_gain, exp_gate, exp_up, exp_down,
+            sh_gate, sh_up, sh_down, out_gain,
         )
 
     placed = (

time: 46.8 us -> 40.9 us (0.87)
  local copies, waits for them, and re-layouts: 6.77 us -> 1.47 us
    unnamed x3 -> x1, local copies, waits for them, and re-layouts: 4.2 us -> 1.47 us
    reshape x2 -> x0, local copies, waits for them, and re-layouts: 2.57 us -> none  [the longest x1 1.29 us: shards(): norm_gain.reshape(1, -1)]
where the time goes in v2:
time: 40.9 us; the launch traced here: 40.8 us
  Pallas kernels  39.3 us (96%)
  local copies, waits for them, and re-layouts  1.47 us (4%)
    pallas_call x1, Pallas kernels, shards(): pl.pallas_call(functools.partial(kernel, n_ep, n_tp, experts), out_shape=...  39.3 us
    unnamed x1, local copies, waits for them, and re-layouts  1.47 us

profile of v2, /device:TPU:0, one launch (start us, length us, event | category | flops | bytes accessed | tf_op | source)
XLA Modules:
  0.0 40.8 jit_solution(2252148676689616494)
XLA Ops:
  0.0 39.3 %shard_map.109 = bf16[32,1024]{1,0:T(8,128)(2,1)} custom-call(bf16[32,2048]{1,0:T(8,128)(2,1)} %tok_ref.1, s32[4,32]{1,0:T(4,128)} %bitcast.2, f32[4,32]{1,0:T(4,128)} %bitcast.3, bf16[2048]{0:T(1024)(128)(2,1)} %ngain_ref.1, bf16[1,2048,1024]{2,1,0:T(8,128)(2,1)} %wg_hbm.1, bf16[1,2048,1024]{2,1,0:T(8,128)(2,1)} %wu_hbm.1, bf16[1,1024,2048]{2,1,0:T(8,128)(2,1)} %wd_hbm.1, ...), custom_call_target="tpu_custom_call" | custom-call | tf_op jit(solution)/shard_map/pallas_call | solution.py:242
  39.3 1.5 %copy.13 = bf16[32,1024]{1,0:T(8,128)(2,1)} copy(bf16[32,1024]{1,0:T(8,128)(2,1)} %shard_map.109) | data formatting | bytes 131072

commit v3 on v2

--- a/solution.py
+++ b/solution.py
@@ -108,7 +108,7 @@
         shid[:, cols] = (silu(g) * u).astype(BF16)
 
     loads[2].wait()
-    dtile = min(256, Dt)
+    dtile = min(512, Dt)
 
     @pl.loop(0, D // dtile)
     def _(i):
@@ -126,7 +126,7 @@
 
     loads[3].wait()
     loads[4].wait()
-    ftile = min(256, F)
+    ftile = min(512, F)
     glane = lax.broadcasted_iota(jnp.int32, (rows, pad), 1)
     mine = (lax.rem(glane, experts) == me) & (glane < 3 * experts)
 
@@ -159,6 +159,7 @@
 
     js = list(range(1, n_tp)) + [0]
     d_copies = {}
+    x_copies = {}
     for j in js:
         def store(src, dst, value):
             d_out[j, :, :, dst] = value.astype(BF16).reshape(nz, T, dtile)
@@ -168,8 +169,6 @@
         copy.start()
         d_copies[j] = copy
 
-    x_copies = {}
-    for j in js:
         def keep(src, dst, value):
             acc[:, :, dst] = value.reshape(nz, T, dtile)
             acc[z, :, dst] += shp[:, src]

time: 40.9 us -> 39.3 us (0.961)
  Pallas kernels: 39.3 us -> 37.7 us
    pallas_call x1, Pallas kernels: 39.3 us -> 37.7 us  [shards(): pl.pallas_call(functools.partial(kernel, n_ep, n_tp, experts), out_shape=...]
where the time goes in v3:
time: 39.3 us; the launch traced here: 39.2 us
  Pallas kernels  37.7 us (96%)
  local copies, waits for them, and re-layouts  1.47 us (4%)
    pallas_call x1, Pallas kernels, shards(): pl.pallas_call(functools.partial(kernel, n_ep, n_tp, experts), out_shape=...  37.7 us
    unnamed x1, local copies, waits for them, and re-layouts  1.47 us

profile of v3, /device:TPU:0, one launch (start us, length us, event | category | flops | bytes accessed | tf_op | source)
XLA Modules:
  0.0 39.2 jit_solution(3172883438966516069)
XLA Ops:
  0.0 37.7 %shard_map.109 = bf16[32,1024]{1,0:T(8,128)(2,1)} custom-call(bf16[32,2048]{1,0:T(8,128)(2,1)} %tok_ref.1, s32[4,32]{1,0:T(4,128)} %bitcast.2, f32[4,32]{1,0:T(4,128)} %bitcast.3, bf16[2048]{0:T(1024)(128)(2,1)} %ngain_ref.1, bf16[1,2048,1024]{2,1,0:T(8,128)(2,1)} %wg_hbm.1, bf16[1,2048,1024]{2,1,0:T(8,128)(2,1)} %wu_hbm.1, bf16[1,1024,2048]{2,1,0:T(8,128)(2,1)} %wd_hbm.1, ...), custom_call_target="tpu_custom_call" | custom-call | tf_op jit(solution)/shard_map/pallas_call | solution.py:241
  37.7 1.5 %copy.13 = bf16[32,1024]{1,0:T(8,128)(2,1)} copy(bf16[32,1024]{1,0:T(8,128)(2,1)} %shard_map.109) | data formatting | bytes 131072
